TPU v7x, 512 devices: a whole 4x4x16 slice. The times are simulated.
512 devices in a mesh: sp: 64 (over z, y), tp: 8 (over x, core).
Axes of the slice: x: 4, y: 4, z: 16, core: 2. Of those that a mesh axis runs over, the one named last changes fastest.
Arguments:
- tokens: bfloat16 [16384, 2048], P('sp', 'tp'), may hold values from -6 to 6
- outer_gate: bfloat16 [2048, 1024], P(None, 'tp'), may hold values from -0.125 to 0.125
- inner_gate: bfloat16 [2048, 1024], P(None, 'tp'), may hold values from -0.125 to 0.125
- conv_input: bfloat16 [2048, 1024], P(None, 'tp'), may hold values from -0.125 to 0.125
- conv_taps: bfloat16 [3, 1024], P(None, 'tp'), may hold values from -3.5 to 3.5
- query_down: bfloat16 [2048, 512], P(None, 'tp'), may hold values from -0.125 to 0.125
- latent_down: bfloat16 [2048, 256], P(None, 'tp'), may hold values from -0.125 to 0.125
- rotary_down: bfloat16 [2048, 32], replicated, may hold values from -5.303301 to 5.303301
- query_gain: float32 [512], replicated, may hold values from 0.1 to 1.9
- latent_gain: float32 [256], replicated, may hold values from 0.1 to 1.9
- query_up: bfloat16 [512, 1536], P(None, 'tp'), may hold values from -0.52734375 to 0.52734375
- latent_up: bfloat16 [256, 2048], P(None, 'tp'), may hold values from -0.75 to 0.75
- conv_project: bfloat16 [1024, 2048], P('tp'), may hold values from -0.1875 to 0.1875
- attend_project: bfloat16 [1024, 2048], P('tp'), may hold values from -0.1875 to 0.1875
Outputs:
- mixed: bfloat16 [16384, 2048], P(('sp', 'tp'))
All inputs are finite; a program needn't handle non-finite values.
Results may differ from a plain program's by a relative error of at most 0.035.
Values may be sent and summed in bfloat16 or wider, within the bound.
No kernel may reach another device: no remote copies, remote signals or barrier semaphores. Data moves between devices by JAX's collectives and lax.ppermute only.
A program may use at most 128 MiB of HBM per device.

v0:
```python
import math

import jax
import jax.numpy as jnp
from jax import lax
from jax.sharding import Mesh
from jax.sharding import PartitionSpec as P

NOPE = 64
ROPE = 32
VDIM = 64
SP = ("sp_0", "sp_1")
SP_TP = ("sp_0", "sp_1", "tp")


neg_fill = -1e30
rotary_base = 10000.0
norm_epsilon = 1e-06


def from_everyone(shard, axis):
    length = lax.axis_size(axis)
    return lax.all_to_all(
        jnp.broadcast_to(shard[None], (length, *shard.shape)), axis, 0, 0, tiled=True
    )


def in_order(tiles, dim):
    tiles = jnp.moveaxis(tiles, 0, dim)
    shape = tiles.shape
    return tiles.reshape(*shape[:dim], shape[dim] * shape[dim + 1], *shape[dim + 2 :])


def gather_directly(shard, axis, dim):
    tiles = from_everyone(shard, axis)
    return in_order(tiles, dim)


def gather_packed(arrays, axis, dims):
    ravelled = jnp.concatenate([a.reshape(-1) for a in arrays])
    lines, at, gathered = (lax.all_gather(ravelled, axis), 0, [])
    for a, dim in zip(arrays, dims):
        tiles = lines[:, at : at + a.size].reshape(-1, *a.shape)
        gathered.append(in_order(tiles, dim))
        at += a.size
    return tuple(gathered)


def shifted(shard, axis, by):
    length = lax.axis_size(axis)
    pairs = [(i, i + by) for i in range(length) if 0 <= i + by < length]
    return lax.ppermute(shard, axis, pairs)


def gather_axes(shard, axes, dim):
    for axis in reversed(axes):
        shard = lax.all_gather(shard, axis, axis=dim, tiled=True)
    return shard


def cut_along(shard, dim, length):
    shape = shard.shape
    tiles = shard.reshape(*shape[:dim], length, shape[dim] // length, *shape[dim + 1 :])
    return jnp.moveaxis(tiles, dim, 0)


def sent_and_summed(shard, axis, dim):
    tiles = cut_along(shard, dim, lax.axis_size(axis))
    arrived = lax.all_to_all(tiles, axis, split_axis=0, concat_axis=0, tiled=True)
    return arrived.astype(jnp.float32).sum(axis=0)


def rotate(values, positions):
    half = values.shape[-1] // 2
    inverse = rotary_base ** (-(jnp.arange(half, dtype=jnp.float32) * 2.0 / (2 * half)))
    angle = positions[:, None] * inverse[None, :]
    if values.ndim == 3:
        angle = angle[:, None, :]
    cosine = jnp.cos(angle)
    sine = jnp.sin(angle)
    first = values[..., :half]
    second = values[..., half:]
    return jnp.concatenate([first * cosine - second * sine, first * sine + second * cosine], -1)


def rms_scale(latent, gain):
    values = latent.astype(jnp.float32)
    factor = lax.rsqrt(jnp.mean(values * values, -1, keepdims=True) + norm_epsilon)
    return (values * factor * gain).astype(jnp.bfloat16)


def local(
    tokens,
    outer_gate,
    inner_gate,
    conv_input,
    conv_taps,
    query_down,
    latent_down,
    rotary_down,
    query_gain,
    latent_gain,
    query_up,
    latent_up,
    conv_project,
    attend_project,
):
    tok_rows = tokens.shape[0]
    groups = lax.axis_size("tp")
    seq_devices = lax.axis_size(SP)
    local_heads = query_up.shape[1] // (NOPE + ROPE)
    weights = (outer_gate, inner_gate, conv_input, query_down, latent_down, rotary_down)
    piece = gather_directly(tokens, "tp", 1)
    outer, inner, signal, query_part, latent_part, rotary_raw = tuple(
        (jnp.dot(piece, weight, preferred_element_type=jnp.float32) for weight in weights)
    )
    query_lat, latent_lat = gather_packed(
        (query_part.astype(jnp.bfloat16), latent_part.astype(jnp.bfloat16)), "tp", (1, 1)
    )
    gated = (inner * signal).astype(jnp.bfloat16)
    reach = conv_taps.shape[0] - 1
    rim = shifted(gated[tok_rows - reach :], SP, 1)
    padded = jnp.concatenate([rim, gated], 0).astype(jnp.float32)
    taps = conv_taps.astype(jnp.float32)
    filtered = padded[0:tok_rows] * taps[0]
    for index in range(1, reach + 1):
        filtered = filtered + padded[index : index + tok_rows] * taps[index]
    conv_result = (outer * filtered).astype(jnp.bfloat16)
    seq_index = lax.axis_index(SP)
    offset = seq_index * tok_rows
    query_index = offset + jnp.arange(tok_rows, dtype=jnp.int32)
    positions = query_index.astype(jnp.float32)
    query_norm = rms_scale(query_lat, query_gain)
    latent_norm = rms_scale(latent_lat, latent_gain)
    rotary_key = rotate(rotary_raw, positions).astype(jnp.bfloat16)
    query_full = jnp.dot(query_norm, query_up, preferred_element_type=jnp.float32)
    query_full = query_full.reshape(tok_rows, local_heads, NOPE + ROPE)
    query_plain = query_full[..., :NOPE].astype(jnp.bfloat16)
    query_rot = rotate(query_full[..., NOPE:], positions).astype(jnp.bfloat16)
    scale = (NOPE + ROPE) ** (-0.5)
    query_sets = ((query_plain, query_rot, query_index),)
    set_lasts = tuple((jnp.max(members[2]) for members in query_sets))
    overall_last = set_lasts[0]

    def update(current, members, key_plain, values, rot_block, first, block):
        plain, turned, indices = members
        best, total, accum = current
        scores = jnp.einsum("qhd,khd->hqk", plain, key_plain, preferred_element_type=jnp.float32)
        scores = scores + jnp.einsum(
            "qhr,kr->hqk", turned, rot_block, preferred_element_type=jnp.float32
        )
        scores = scores * scale
        key_index = first + jnp.arange(block, dtype=jnp.int32)
        visible = key_index[None, :] <= indices[:, None]
        scores = jnp.where(visible[None], scores, neg_fill)
        new_best = jnp.maximum(best, jnp.max(scores, -1))
        factor = jnp.exp(best - new_best)
        weight = jnp.exp(scores - new_best[..., None])
        total = total * factor + jnp.sum(weight, -1)
        accum = accum * factor[..., None] + jnp.einsum(
            "hqk,khd->hqd", weight.astype(jnp.bfloat16), values, preferred_element_type=jnp.float32
        )
        return (new_best, total, accum)

    initial = tuple(
        (
            (
                jnp.full((local_heads, members[2].shape[0]), neg_fill, jnp.float32),
                jnp.zeros((local_heads, members[2].shape[0]), jnp.float32),
                jnp.zeros((local_heads, members[2].shape[0], VDIM), jnp.float32),
            )
            for members in query_sets
        )
    )
    share = tok_rows // groups
    lower = lax.axis_index("tp") * share
    own_keys = jnp.concatenate(
        [
            lax.dynamic_slice_in_dim(latent_norm, lower, share, 0),
            lax.dynamic_slice_in_dim(rotary_key, lower, share, 0),
        ],
        -1,
    )
    seq_keys = gather_axes(own_keys[None], SP, 0)
    all_keys = lax.all_gather(seq_keys, "tp", axis=1, tiled=True)
    all_keys = all_keys.reshape(seq_devices * tok_rows, own_keys.shape[1])
    latent_width = latent_norm.shape[1]
    carry = initial
    keys_latent = all_keys[:, :latent_width]
    keys_rot = all_keys[:, latent_width:]
    count = keys_latent.shape[0]
    block = math.gcd(count, 512)
    latent_blocks = keys_latent.reshape(count // block, block, keys_latent.shape[1])
    rot_blocks = keys_rot.reshape(count // block, block, keys_rot.shape[1])

    def advance(states, inputs):
        latent_block, rot_block, number = inputs
        first = 0 + number * block

        def compute(current):
            expanded = jnp.dot(latent_block, latent_up, preferred_element_type=jnp.float32)
            expanded = expanded.astype(jnp.bfloat16).reshape(block, local_heads, NOPE + VDIM)
            key_plain = expanded[..., :NOPE]
            values = expanded[..., NOPE:]
            results = []
            for members, last, state in zip(query_sets, set_lasts, current):
                results.append(
                    lax.cond(
                        first > last,
                        lambda kept: kept,
                        lambda kept, members=members: update(
                            kept, members, key_plain, values, rot_block, first, block
                        ),
                        state,
                    )
                )
            return tuple(results)

        return (lax.cond(first > overall_last, lambda current: current, compute, states), None)

    numbers = jnp.arange(count // block, dtype=jnp.int32)
    carry, unused = lax.scan(advance, carry, (latent_blocks, rot_blocks, numbers))
    states = carry
    outputs = []
    for state in states:
        best, total, accum = state
        rows = accum.shape[1]
        outputs.append(
            (accum / total[..., None])
            .transpose(1, 0, 2)
            .reshape(rows, local_heads * VDIM)
            .astype(jnp.bfloat16)
        )
    attended = outputs[0]
    mixed = sent_and_summed(
        (
            jnp.dot(conv_result, conv_project, preferred_element_type=jnp.float32)
            + jnp.dot(attended, attend_project, preferred_element_type=jnp.float32)
        ).astype(jnp.bfloat16),
        "tp",
        0,
    )
    return mixed.astype(jnp.bfloat16)


def solution(mesh):
    split = Mesh(mesh.devices.reshape(16, 4, mesh.shape["tp"]), ("sp_0", "sp_1", "tp"))
    in_specs = (
        P(SP, "tp"),
        P(None, "tp"),
        P(None, "tp"),
        P(None, "tp"),
        P(None, "tp"),
        P(None, "tp"),
        P(None, "tp"),
        P(),
        P(),
        P(),
        P(None, "tp"),
        P(None, "tp"),
        P("tp", None),
        P("tp", None),
    )
    out_specs = P(SP_TP, None)
    return jax.shard_map(local, mesh=split, in_specs=in_specs, out_specs=out_specs, check_vma=False)
```

profile of v0, /device:TPU:504, one launch (start us, length us, event | category | flops | bytes accessed | tf_op | source)
XLA Modules:
  0.0 442.9 jit_solution(10896540018394202461)
XLA Ops:
  13.2 15.9 %all-to-all-done = bf16[8,256,256]{1,2,0:T(8,128)(2,1)S(1)} async-done(((bf16[8,256,256]{1,2,0:T(8,128)(2,1)}), bf16[8,256,256]{1,2,0:T(8,128)(2,1)S(1)}, u32[]{:S(2)}, u32[]{:S(2)}) %all-to-all-start) | async-done | bytes 1048608 | tf_op jit(solution)/shard_map/all_to_all | solution.py:23
  30.1 13.0 %all-gather = bf16[196608]{0:T(1024)(128)(2,1)S(1)} all-gather(bf16[24576]{0:T(1024)(128)(2,1)S(1)} %pad_maximum_fusion), channel_id=2, replica_groups=mesh['sp_0'=16,'sp_1'=4,'tp'=8] {'tp'}, dimensions={0}, use_global_device_ids=true | all-gather | bytes 442368 | tf_op jit(solution)/shard_map/all_gather | solution.py:41
  45.2 12.7 %all-gather.1 = bf16[128,288]{1,0:T(8,128)(2,1)} all-gather(bf16[32,288]{1,0:T(8,128)(2,1)S(1)} %pad_maximum_fusion.2), channel_id=3, replica_groups=mesh['sp_0'=16,'sp_1'=4,'tp'=8] {'sp_1'}, dimensions={0}, use_global_device_ids=true | all-gather | bytes 92160 | tf_op jit(solution)/shard_map/all_gather | solution.py:57
  58.0 67.6 %all-gather.5.cloned.1.call-done = bf16[64,32,288]{2,1,0:T(8,128)(2,1)} async-done(((bf16[4,32,288]{2,1,0:T(8,128)(2,1)}), bf16[64,32,288]{2,1,0:T(8,128)(2,1)}) %all-gather.5.cloned.1.call-update) | async-done | bytes 1179664 | tf_op jit(solution)/shard_map/all_gather | solution.py:57
  138.2 62.9 %all-gather.7.cloned.1.call-done = bf16[64,256,288]{2,1,0:T(8,128)(2,1)} async-done(((bf16[64,32,288]{2,1,0:T(8,128)(2,1)}), bf16[64,256,288]{2,1,0:T(8,128)(2,1)}) %all-gather.7.cloned.1.call-update) | async-done | bytes 9437200 | tf_op jit(solution)/shard_map/all_gather | solution.py:185
  201.1 7.0 %slice.89 = bf16[16384,256]{1,0:T(8,128)(2,1)} slice(bf16[16384,288]{1,0:T(8,128)(2,1)} %bitcast.77), slice={[0:16384], [0:256]} | slice | bytes 16777216 | tf_op jit(solution)/shard_map/slice | solution.py:189
  211.9 4.6 %copy.50 = bf16[32,512,32]{1,2,0:T(8,128)(2,1)} copy(bf16[32,512,32]{2,1,0:T(8,128)(2,1)} %bitcast.76) | data formatting | bytes 2097152
  216.5 198.0 %while.15 = (s32[]{:T(128)}, f32[2,256]{1,0:T(2,128)S(1)}, f32[2,256]{1,0:T(2,128)S(1)}, f32[2,256,64]{1,2,0:T(8,128)S(1)}, s32[32]{0:T(128)S(1)}, /*index=5*/s3...) while((s32[]{:T(128)}, f32[2,256]{1,0:T(2,128)S(1)}, ...), condition=%wide.region_11.12_spmd.clone, body=%wide.region_4.11_spmd.clone.sunk | while | flops 153421568 | bytes 7382473 | solution.py:222
  224.4 4.5 %conditional.4 = ((f32[2,256]{1,0:T(2,128)S(1)}, f32[2,256]{1,0:T(2,128)S(1)}, f32[2,256,64]{1,2,0:T(8,128)S(1)})) conditional(s32[]{:T(128)} %convert_element_type.147, (s32[]{:T(128)}, s32[]{:T(128)}, bf16[32,512,256]{2,1,0:T(8,128)(2,1)}, s32[]{:T(128)}, bf16[256,256]{1,0:T(8,128)(2,1)S(1)}, /*index=5*/s32[]{:T(128)}, ...), branch_computations={%region_5.9_spmd, %region_10.10_spmd} | conditional | flops 153421568 | bytes 7377054 | solution.py:219
  230.6 4.5 %conditional.4 = ((f32[2,256]{1,0:T(2,128)S(1)}, f32[2,256]{1,0:T(2,128)S(1)}, f32[2,256,64]{1,2,0:T(8,128)S(1)})) conditional(s32[]{:T(128)} %convert_element_type.147, (s32[]{:T(128)}, s32[]{:T(128)}, bf16[32,512,256]{2,1,0:T(8,128)(2,1)}, s32[]{:T(128)}, bf16[256,256]{1,0:T(8,128)(2,1)S(1)}, /*index=5*/s32[]{:T(128)}, ...), branch_computations={%region_5.9_spmd, %region_10.10_spmd} | conditional | flops 153421568 | bytes 7377054 | solution.py:219
  236.8 4.5 %conditional.4 = ((f32[2,256]{1,0:T(2,128)S(1)}, f32[2,256]{1,0:T(2,128)S(1)}, f32[2,256,64]{1,2,0:T(8,128)S(1)})) conditional(s32[]{:T(128)} %convert_element_type.147, (s32[]{:T(128)}, s32[]{:T(128)}, bf16[32,512,256]{2,1,0:T(8,128)(2,1)}, s32[]{:T(128)}, bf16[256,256]{1,0:T(8,128)(2,1)S(1)}, /*index=5*/s32[]{:T(128)}, ...), branch_computations={%region_5.9_spmd, %region_10.10_spmd} | conditional | flops 153421568 | bytes 7377054 | solution.py:219
  255.4 4.5 %conditional.4 = ((f32[2,256]{1,0:T(2,128)S(1)}, f32[2,256]{1,0:T(2,128)S(1)}, f32[2,256,64]{1,2,0:T(8,128)S(1)})) conditional(s32[]{:T(128)} %convert_element_type.147, (s32[]{:T(128)}, s32[]{:T(128)}, bf16[32,512,256]{2,1,0:T(8,128)(2,1)}, s32[]{:T(128)}, bf16[256,256]{1,0:T(8,128)(2,1)S(1)}, /*index=5*/s32[]{:T(128)}, ...), branch_computations={%region_5.9_spmd, %region_10.10_spmd} | conditional | flops 153421568 | bytes 7377054 | solution.py:219
  261.6 4.5 %conditional.4 = ((f32[2,256]{1,0:T(2,128)S(1)}, f32[2,256]{1,0:T(2,128)S(1)}, f32[2,256,64]{1,2,0:T(8,128)S(1)})) conditional(s32[]{:T(128)} %convert_element_type.147, (s32[]{:T(128)}, s32[]{:T(128)}, bf16[32,512,256]{2,1,0:T(8,128)(2,1)}, s32[]{:T(128)}, bf16[256,256]{1,0:T(8,128)(2,1)S(1)}, /*index=5*/s32[]{:T(128)}, ...), branch_computations={%region_5.9_spmd, %region_10.10_spmd} | conditional | flops 153421568 | bytes 7377054 | solution.py:219
  267.7 4.5 %conditional.4 = ((f32[2,256]{1,0:T(2,128)S(1)}, f32[2,256]{1,0:T(2,128)S(1)}, f32[2,256,64]{1,2,0:T(8,128)S(1)})) conditional(s32[]{:T(128)} %convert_element_type.147, (s32[]{:T(128)}, s32[]{:T(128)}, bf16[32,512,256]{2,1,0:T(8,128)(2,1)}, s32[]{:T(128)}, bf16[256,256]{1,0:T(8,128)(2,1)S(1)}, /*index=5*/s32[]{:T(128)}, ...), branch_computations={%region_5.9_spmd, %region_10.10_spmd} | conditional | flops 153421568 | bytes 7377054 | solution.py:219
  286.3 4.5 %conditional.4 = ((f32[2,256]{1,0:T(2,128)S(1)}, f32[2,256]{1,0:T(2,128)S(1)}, f32[2,256,64]{1,2,0:T(8,128)S(1)})) conditional(s32[]{:T(128)} %convert_element_type.147, (s32[]{:T(128)}, s32[]{:T(128)}, bf16[32,512,256]{2,1,0:T(8,128)(2,1)}, s32[]{:T(128)}, bf16[256,256]{1,0:T(8,128)(2,1)S(1)}, /*index=5*/s32[]{:T(128)}, ...), branch_computations={%region_5.9_spmd, %region_10.10_spmd} | conditional | flops 153421568 | bytes 7377054 | solution.py:219
  298.7 4.5 %conditional.4 = ((f32[2,256]{1,0:T(2,128)S(1)}, f32[2,256]{1,0:T(2,128)S(1)}, f32[2,256,64]{1,2,0:T(8,128)S(1)})) conditional(s32[]{:T(128)} %convert_element_type.147, (s32[]{:T(128)}, s32[]{:T(128)}, bf16[32,512,256]{2,1,0:T(8,128)(2,1)}, s32[]{:T(128)}, bf16[256,256]{1,0:T(8,128)(2,1)S(1)}, /*index=5*/s32[]{:T(128)}, ...), branch_computations={%region_5.9_spmd, %region_10.10_spmd} | conditional | flops 153421568 | bytes 7377054 | solution.py:219
  317.2 4.5 %conditional.4 = ((f32[2,256]{1,0:T(2,128)S(1)}, f32[2,256]{1,0:T(2,128)S(1)}, f32[2,256,64]{1,2,0:T(8,128)S(1)})) conditional(s32[]{:T(128)} %convert_element_type.147, (s32[]{:T(128)}, s32[]{:T(128)}, bf16[32,512,256]{2,1,0:T(8,128)(2,1)}, s32[]{:T(128)}, bf16[256,256]{1,0:T(8,128)(2,1)S(1)}, /*index=5*/s32[]{:T(128)}, ...), branch_computations={%region_5.9_spmd, %region_10.10_spmd} | conditional | flops 153421568 | bytes 7377054 | solution.py:219
  329.6 4.5 %conditional.4 = ((f32[2,256]{1,0:T(2,128)S(1)}, f32[2,256]{1,0:T(2,128)S(1)}, f32[2,256,64]{1,2,0:T(8,128)S(1)})) conditional(s32[]{:T(128)} %convert_element_type.147, (s32[]{:T(128)}, s32[]{:T(128)}, bf16[32,512,256]{2,1,0:T(8,128)(2,1)}, s32[]{:T(128)}, bf16[256,256]{1,0:T(8,128)(2,1)S(1)}, /*index=5*/s32[]{:T(128)}, ...), branch_computations={%region_5.9_spmd, %region_10.10_spmd} | conditional | flops 153421568 | bytes 7377054 | solution.py:219
  348.2 4.5 %conditional.4 = ((f32[2,256]{1,0:T(2,128)S(1)}, f32[2,256]{1,0:T(2,128)S(1)}, f32[2,256,64]{1,2,0:T(8,128)S(1)})) conditional(s32[]{:T(128)} %convert_element_type.147, (s32[]{:T(128)}, s32[]{:T(128)}, bf16[32,512,256]{2,1,0:T(8,128)(2,1)}, s32[]{:T(128)}, bf16[256,256]{1,0:T(8,128)(2,1)S(1)}, /*index=5*/s32[]{:T(128)}, ...), branch_computations={%region_5.9_spmd, %region_10.10_spmd} | conditional | flops 153421568 | bytes 7377054 | solution.py:219
  360.5 4.5 %conditional.4 = ((f32[2,256]{1,0:T(2,128)S(1)}, f32[2,256]{1,0:T(2,128)S(1)}, f32[2,256,64]{1,2,0:T(8,128)S(1)})) conditional(s32[]{:T(128)} %convert_element_type.147, (s32[]{:T(128)}, s32[]{:T(128)}, bf16[32,512,256]{2,1,0:T(8,128)(2,1)}, s32[]{:T(128)}, bf16[256,256]{1,0:T(8,128)(2,1)S(1)}, /*index=5*/s32[]{:T(128)}, ...), branch_computations={%region_5.9_spmd, %region_10.10_spmd} | conditional | flops 153421568 | bytes 7377054 | solution.py:219
  379.1 4.5 %conditional.4 = ((f32[2,256]{1,0:T(2,128)S(1)}, f32[2,256]{1,0:T(2,128)S(1)}, f32[2,256,64]{1,2,0:T(8,128)S(1)})) conditional(s32[]{:T(128)} %convert_element_type.147, (s32[]{:T(128)}, s32[]{:T(128)}, bf16[32,512,256]{2,1,0:T(8,128)(2,1)}, s32[]{:T(128)}, bf16[256,256]{1,0:T(8,128)(2,1)S(1)}, /*index=5*/s32[]{:T(128)}, ...), branch_computations={%region_5.9_spmd, %region_10.10_spmd} | conditional | flops 153421568 | bytes 7377054 | solution.py:219
  391.5 4.5 %conditional.4 = ((f32[2,256]{1,0:T(2,128)S(1)}, f32[2,256]{1,0:T(2,128)S(1)}, f32[2,256,64]{1,2,0:T(8,128)S(1)})) conditional(s32[]{:T(128)} %convert_element_type.147, (s32[]{:T(128)}, s32[]{:T(128)}, bf16[32,512,256]{2,1,0:T(8,128)(2,1)}, s32[]{:T(128)}, bf16[256,256]{1,0:T(8,128)(2,1)S(1)}, /*index=5*/s32[]{:T(128)}, ...), branch_computations={%region_5.9_spmd, %region_10.10_spmd} | conditional | flops 153421568 | bytes 7377054 | solution.py:219
  410.0 4.5 %conditional.4 = ((f32[2,256]{1,0:T(2,128)S(1)}, f32[2,256]{1,0:T(2,128)S(1)}, f32[2,256,64]{1,2,0:T(8,128)S(1)})) conditional(s32[]{:T(128)} %convert_element_type.147, (s32[]{:T(128)}, s32[]{:T(128)}, bf16[32,512,256]{2,1,0:T(8,128)(2,1)}, s32[]{:T(128)}, bf16[256,256]{1,0:T(8,128)(2,1)S(1)}, /*index=5*/s32[]{:T(128)}, ...), branch_computations={%region_5.9_spmd, %region_10.10_spmd} | conditional | flops 153421568 | bytes 7377054 | solution.py:219
  416.1 19.2 %all_to_all.10 = bf16[8,32,2048]{2,1,0:T(8,128)(2,1)S(1)} all-to-all(bf16[8,32,2048]{2,1,0:T(8,128)(2,1)S(1)} %bitcast.80), channel_id=1, replica_groups=mesh['sp_0'=16,'sp_1'=4,'tp'=8] {'tp'}, dimensions={0} | all-to-all | bytes 2097152 | tf_op jit(solution)/shard_map/all_to_all | solution.py:69
  (580 shorter events, 332.3 us)
Async XLA Ops:
  6.5 129.4 %copy-start = (bf16[128,2048]{1,0:T(8,128)(2,1)S(1)}, bf16[128,2048]{1,0:T(8,128)(2,1)}, u32[]{:S(2)}) copy-start(bf16[128,2048]{1,0:T(8,128)(2,1)} %param.32) | copy-start | bytes 1572868
  6.5 22.5 %copy-start.4 = (bf16[2048,64]{0,1:T(8,128)(2,1)S(1)}, bf16[2048,64]{0,1:T(8,128)(2,1)}, u32[]{:S(2)}) copy-start(bf16[2048,64]{0,1:T(8,128)(2,1)} %param.25) | copy-start | bytes 786436
  8.7 20.9 %copy-start.6 = (bf16[2048,32]{0,1:T(8,128)(2,1)S(1)}, bf16[2048,32]{0,1:T(8,128)(2,1)}, u32[]{:S(2)}) copy-start(bf16[2048,32]{0,1:T(8,128)(2,1)} %param.26) | copy-start | bytes 393220
  8.7 20.4 %all-to-all-start = ((bf16[8,256,256]{1,2,0:T(8,128)(2,1)}), bf16[8,256,256]{1,2,0:T(8,128)(2,1)S(1)}, u32[]{:S(2)}, u32[]{:S(2)}) async-start(bf16[8,256,256]{1,2,0:T(8,128)(2,1)} %broadcast_in_dim.22), calls=%async_computation | async-start | bytes 2097152 | tf_op jit(solution)/shard_map/all_to_all | solution.py:23
  13.1 112.5 %all-gather.5.cloned.1.call-start = ((), (), s32[]{:S(2)}) async-start(), calls=%async_computation.2 | async-start | bytes 1671168 | tf_op jit(solution)/shard_map/all_gather | solution.py:57
  29.0 14.3 %copy-start.7 = (bf16[2048,32]{0,1:T(8,128)(2,1)S(1)}, bf16[2048,32]{0,1:T(8,128)(2,1)}, u32[]{:S(2)}) copy-start(bf16[2048,32]{0,1:T(8,128)(2,1)} %param.27) | copy-start | bytes 393220
  43.4 1.3 copy-start.9
  44.3 81.9 %copy-start.8 = (f32[512]{0:T(512)S(1)}, f32[512]{0:T(512)}, u32[]{:S(2)}) copy-start(f32[512]{0:T(512)} %param.28) | copy-start | bytes 6148
  44.3 82.0 %copy-start.10 = (bf16[3,128]{1,0:T(4,128)(2,1)S(1)}, bf16[3,128]{1,0:T(4,128)(2,1)}, u32[]{:S(2)}) copy-start(bf16[3,128]{1,0:T(4,128)(2,1)} %param.24) | copy-start | bytes 2308
  57.9 143.2 %all-gather.7.cloned.1.call-start = ((), (), s32[]{:S(2)}) async-start(), calls=%async_computation.3 | async-start | bytes 14155776 | tf_op jit(solution)/shard_map/all_gather | solution.py:185
  127.1 4.6 %copy-start.5 = (bf16[512,192]{0,1:T(8,128)(2,1)S(1)}, bf16[512,192]{0,1:T(8,128)(2,1)}, u32[]{:S(2)}) copy-start(bf16[512,192]{0,1:T(8,128)(2,1)} %param.30) | copy-start | bytes 589828
  127.4 8.6 %copy-start.3 = (bf16[2048,128]{1,0:T(8,128)(2,1)S(1)}, bf16[2048,128]{1,0:T(8,128)(2,1)}, u32[]{:S(2)}) copy-start(bf16[2048,128]{1,0:T(8,128)(2,1)} %param.21) | copy-start | bytes 1572868
  130.5 5.5 %collective-permute-start = (bf16[2,128]{1,0:T(2,128)(2,1)S(1)}, bf16[2,128]{1,0:T(2,128)(2,1)S(1)}, u32[]{:S(2)}, u32[]{:S(2)}) collective-permute-start(bf16[2,128]{1,0:T(2,128)(2,1)S(1)} %slice.82), channel_id=1, source_target_pairs={{0,8},{8,16},{16,24},{24,32},{32,40},{40,48},{48,56},{56,64},{64,7... | collective-permute-start | bytes 1544 | tf_op jit(solution)/shard_map/ppermute | solution.py:52
  211.9 4.6 %copy-start.2 = (bf16[256,256]{1,0:T(8,128)(2,1)S(1)}, bf16[256,256]{1,0:T(8,128)(2,1)}, u32[]{:S(2)}) copy-start(bf16[256,256]{1,0:T(8,128)(2,1)} %param.31) | copy-start | bytes 393220
  216.5 198.1 %copy-start.1 = (f32[256,2048]{1,0:T(8,128)S(1)}, f32[256,2048]{1,0:T(8,128)}, u32[]{:S(2)}) copy-start(f32[256,2048]{1,0:T(8,128)} %fusion.21) | copy-start | bytes 6291460
Sparse Core Ops, SparseCore 0:
  58.0 67.4 all-gather.4
  127.7 73.3 all-gather.6
where the time goes:
time: 447 us; the launch traced here: 443 us
  waiting for transfers between devices  150 us (34%)
  matrix products  111 us (25%)
  loops' own time  57 us (13%)
  blocking collectives  44.8 us (10%)
  local copies, waits for them, and re-layouts  42.2 us (9%)
  other arithmetic  18 us (4%)
  between operations  13.8 us (3%)
  starting transfers between devices  5.8 us (1%)
    all_gather x1, waiting for transfers between devices, gather_axes(): shard = lax.all_gather(shard, axis, axis=dim, tiled=True)  67.6 us
    all_gather x1, waiting for transfers between devices, local(): all_keys = lax.all_gather(seq_keys, 'tp', axis=1, tiled=True)  62.9 us
    dot_general x32, matrix products, update(): jnp.einsum('qhr,kr->hqk', turned, rot_block, preferred_element_type=jnp.f...  39.9 us
    dot_general x32, matrix products, compute(): jnp.dot(latent_block, latent_up, preferred_element_type=jnp.float32)  37.7 us
    another operation x1, loops' own time, local(): lax.scan(advance, carry, (latent_blocks, rot_blocks, numbers))  36.5 us
    all_to_all x1, blocking collectives, sent_and_summed(): lax.all_to_all(tiles, axis, split_axis=0, concat_axis=0, tiled=True)  19.2 us
    another operation x32, loops' own time, advance(): lax.cond(first > overall_last, lambda current: current, compute, states)  19 us
    dynamic_slice x32, local copies, waits for them, and re-layouts, local(): lax.scan(advance, carry, (latent_blocks, rot_blocks, numbers))  17.7 us
  transfers between devices with their start and end apart: 4, of which 4 were waited for; matrix products, arithmetic and copies ran while one was open for 2% of the time, Pallas kernels for 0%

commit v1 on v0

v1 whole, which is shorter than its diff:
```python
import math

import jax
import jax.numpy as jnp
from jax import lax
from jax.experimental import pallas as pl
from jax.experimental.pallas import tpu as pltpu
from jax.sharding import Mesh
from jax.sharding import PartitionSpec as P

NOPE = 64
ROPE = 32
VDIM = 64
SP = ("sp_0", "sp_1")
SP_TP = ("sp_0", "sp_1", "tp")
NZ = 16
NY = 4
ROWS = 256
HEADS = 2
CHUNK = 4
STATS = 16
Y_SHIFTS = (0, 1, 3, 2)
X_SHIFTS = (0, 1, 3, 2)

neg_fill = -1e30
rotary_base = 10000.0
norm_epsilon = 1e-06
bf16 = jnp.bfloat16
f32 = jnp.float32
VMEM = pl.BlockSpec(memory_space=pltpu.VMEM)
SMEM = pl.BlockSpec(memory_space=pltpu.SMEM)


def params():
    return pltpu.CompilerParams(vmem_limit_bytes=48 * 1024 * 1024)


def cost(flops):
    return pl.CostEstimate(flops=flops, bytes_accessed=4 * 1024 * 1024, transcendentals=0)


def dot(a, b):
    return jnp.dot(a, b, preferred_element_type=f32)


def latents_kernel(tok, wl, wr, wq, cos, sin, kr_out, q_out):
    groups, rows, width = tok.shape
    lat = jnp.zeros((rows, wl.shape[1]), f32)
    rot = jnp.zeros((rows, wr.shape[1]), f32)
    qry = jnp.zeros((rows, wq.shape[1]), f32)
    for g in range(groups):
        piece = tok[g]
        span = pl.ds(g * width, width)
        lat = lat + dot(piece, wl[span, :])
        rot = rot + dot(piece, wr[span, :])
        qry = qry + dot(piece, wq[span, :])
    both = jnp.concatenate([lat, rot, qry], 1).T
    half = ROPE // 2
    a = both[32 : 32 + half]
    b = both[32 + half : 64]
    c = cos[...]
    s = sin[...]
    kr_out[...] = jnp.concatenate([both[:32], a * c - b * s, a * s + b * c], 0).astype(bf16)
    q_out[...] = both[64:].astype(bf16)


def gates_kernel(tok, wo, wi, ws, outer_out, gated_out):
    groups, rows, width = tok.shape
    outer = jnp.zeros((rows, wo.shape[1]), f32)
    inner = outer
    signal = outer
    for g in range(groups):
        piece = tok[g]
        span = pl.ds(g * width, width)
        outer = outer + dot(piece, wo[span, :])
        inner = inner + dot(piece, wi[span, :])
        signal = signal + dot(piece, ws[span, :])
    outer_out[...] = outer
    gated_out[...] = (inner * signal).astype(bf16)


def normed(lat, gain):
    factor = lax.rsqrt(jnp.mean(lat * lat, 0, keepdims=True) + norm_epsilon)
    return (lat * factor * gain).astype(bf16)


def attention_kernel(where, *refs):
    lats = refs[:8]
    gathered, wq, wk, gq, gk, cos, sin, out, q_s, k_s, v_s, acc_s, m_s = refs[8:]
    z = where[0]
    y = where[1]
    per = NOPE + ROPE
    half = ROPE // 2
    scale = per ** (-0.5) * math.log2(math.e)
    for j in range(NY):
        base = NZ * 32 + 64 * j
        lat = jnp.concatenate([a[base : base + 64, :] for a in lats], 0).astype(f32)
        full = dot(wq[...], normed(lat, gq[...])) * scale
        c = cos[:, ROWS * j : ROWS * (j + 1)]
        s = sin[:, ROWS * j : ROWS * (j + 1)]
        for h in range(HEADS):
            at = per * h
            a = full[at + NOPE : at + NOPE + half]
            b = full[at + NOPE + half : at + per]
            q_s[h, j] = jnp.concatenate(
                [full[at : at + NOPE], a * c - b * s, a * s + b * c], 0
            ).astype(bf16)
            m_s[h, j] = jnp.full((8, ROWS), neg_fill, f32)
            acc_s[h, j] = jnp.zeros((VDIM + 16, ROWS), f32)
    for h in range(HEADS):
        v_s[h, VDIM:, :] = jnp.ones((16, CHUNK * ROWS), bf16)

    def chunk(number, masked):
        for b in range(CHUNK):
            zz = number * CHUNK + b
            start = pl.multiple_of(zz * 32, 32)
            lat = jnp.concatenate([a[pl.ds(start, 32), :] for a in lats], 0).astype(f32)
            full = dot(wk[...], normed(lat, gk[...])).astype(bf16)
            rot = gathered[zz, 32:64, :].astype(f32)
            for h in range(HEADS):
                at = (NOPE + VDIM) * h
                tall = jnp.concatenate([full[at : at + NOPE].astype(f32), rot], 0)
                k_s[h, ROWS * b : ROWS * (b + 1), :] = tall.T.astype(bf16)
                v_s[h, :VDIM, ROWS * b : ROWS * (b + 1)] = full[at + NOPE : at + NOPE + VDIM]
        for h in range(HEADS):
            for j in range(NY):
                scores = dot(k_s[h], q_s[h, j])
                if masked:
                    key = lax.broadcasted_iota(jnp.int32, (CHUNK * ROWS, ROWS), 0)
                    col = lax.broadcasted_iota(jnp.int32, (CHUNK * ROWS, ROWS), 1)
                    yq = lax.rem(y + NY - Y_SHIFTS[j], NY)
                    ahead = (z - number * CHUNK) * (NY * ROWS) + (yq - y) * ROWS
                    block = lax.shift_right_logical(key, 8)
                    scores = jnp.where(
                        key + block * (NY * ROWS - ROWS) - col <= ahead, scores, neg_fill
                    )
                old = m_s[h, j, 0:1, :]
                best = jnp.maximum(old, jnp.max(scores, 0, keepdims=True))
                weight = jnp.exp2(scores - best).astype(bf16)
                acc_s[h, j] = acc_s[h, j] * jnp.exp2(old - best) + dot(v_s[h], weight)
                m_s[h, j, 0:1, :] = best

    last = z // CHUNK

    def step(number, carry):
        chunk(number, False)
        return carry

    lax.fori_loop(0, last, step, 0)
    chunk(last, True)
    row = lax.broadcasted_iota(jnp.int32, (STATS, ROWS), 0)
    for j in range(NY):
        yq = lax.rem(y + NY - Y_SHIFTS[j], NY)
        stats = jnp.zeros((STATS, ROWS), f32)
        for h in range(HEADS):
            acc = acc_s[h, j]
            total = acc[VDIM : VDIM + 1]
            out[yq, VDIM * h : VDIM * (h + 1), :] = (acc[:VDIM] / total).astype(bf16)
            rest = m_s[h, j, 0:1, :] + jnp.log2(total)
            for part in range(3):
                piece = rest.astype(bf16).astype(f32)
                stats = jnp.where(row == 3 * h + part, piece, stats)
                rest = rest - piece
        out[yq, HEADS * VDIM :, :] = stats.astype(bf16)


def project_kernel(parts, outer, gated, rim, taps, wc, wa, out):
    rows, width = gated.shape
    mixed = []
    for h in range(HEADS):
        at = HEADS * VDIM
        logs = []
        for p in range(NY):
            stat = parts[p, at : at + STATS, :].astype(f32)
            logs.append(stat[3 * h : 3 * h + 1] + stat[3 * h + 1 : 3 * h + 2] + stat[3 * h + 2 : 3 * h + 3])
        best = jnp.maximum(jnp.maximum(logs[0], logs[1]), jnp.maximum(logs[2], logs[3]))
        total = jnp.zeros_like(best)
        summed = jnp.zeros((VDIM, rows), f32)
        for p in range(NY):
            weight = jnp.exp2(logs[p] - best)
            total = total + weight
            summed = summed + parts[p, VDIM * h : VDIM * (h + 1), :].astype(f32) * weight
        mixed.append(summed / total)
    attended = jnp.concatenate(mixed, 0).T.astype(bf16)
    here = gated[...].astype(f32)
    before = rim[...].astype(f32)
    row = lax.broadcasted_iota(jnp.int32, (rows, width), 0)
    one = jnp.where(row == 0, before[1:2], pltpu.roll(here, 1, 0))
    two = pltpu.roll(here, 2, 0)
    two = jnp.where(row == 0, before[0:1], jnp.where(row == 1, before[1:2], two))
    tap = taps[...].astype(f32)
    filtered = two * tap[0:1] + one * tap[1:2] + here * tap[2:3]
    conv = (outer[...] * filtered).astype(bf16)
    both = jnp.concatenate([conv, attended], 1)
    weights = jnp.concatenate([wc[...], wa[...]], 0)
    out[...] = dot(both, weights).astype(bf16)


def call(kernel, outs, flops, scratch=(), scalars=0):
    def run(*arrays):
        return pl.pallas_call(
            kernel,
            out_shape=outs,
            in_specs=[SMEM] * scalars + [VMEM] * (len(arrays) - scalars),
            out_specs=jax.tree.map(lambda _: VMEM, outs),
            scratch_shapes=list(scratch),
            compiler_params=params(),
            cost_estimate=cost(flops),
        )(*arrays)

    return run


def along_x(value, by):
    return lax.ppermute(value, "tp", [(i, (i + 2 * by) % 8) for i in range(8)])


def to_partner(value):
    return lax.ppermute(value, "tp", [(i, i ^ 1) for i in range(8)])


def along_y(value, by):
    return lax.ppermute(value, "sp_1", [(i, (i + by) % NY) for i in range(NY)])


def local(
    tokens,
    outer_gate,
    inner_gate,
    conv_input,
    conv_taps,
    query_down,
    latent_down,
    rotary_down,
    query_gain,
    latent_gain,
    query_up,
    latent_up,
    conv_project,
    attend_project,
):
    rows = tokens.shape[0]
    groups = lax.axis_size("tp")
    z = lax.axis_index("sp_0")
    y = lax.axis_index("sp_1")
    tp = lax.axis_index("tp")
    shapes = jax.ShapeDtypeStruct
    everyone = jnp.broadcast_to(tokens[None], (groups, *tokens.shape))
    pieces = lax.all_to_all(everyone, "tp", 0, 0, tiled=True)

    y_order = (y - jnp.array(Y_SHIFTS, jnp.int32)) % NY
    starts = (z * NY + y_order) * rows
    positions = (starts[:, None] + jnp.arange(rows, dtype=jnp.int32)[None]).reshape(-1).astype(f32)
    half = ROPE // 2
    inverse = rotary_base ** (-(jnp.arange(half, dtype=f32) * 2.0 / (2 * half)))
    angle = inverse[:, None] * positions[None, :]
    cosine = jnp.cos(angle)
    sine = jnp.sin(angle)
    x_order = (tp // 2 - jnp.array(X_SHIFTS, jnp.int32)) % 4
    order = jnp.concatenate([x_order * 2 + tp % 2, x_order * 2 + 1 - tp % 2])
    wq = jnp.take(query_up.reshape(8, 64, -1), order, axis=0).reshape(512, -1).T
    wk = jnp.take(latent_up.reshape(8, 32, -1), order, axis=0).reshape(256, -1).T
    gq = jnp.take(query_gain.reshape(8, 64), order, axis=0).reshape(512, 1)
    gk = jnp.take(latent_gain.reshape(8, 32), order, axis=0).reshape(256, 1)

    own_kr, own_q = call(
        latents_kernel, (shapes((64, rows), bf16), shapes((64, rows), bf16)), 2 * 256 * 2048 * 128
    )(pieces, latent_down, rotary_down, query_down, cosine[:, :rows], sine[:, :rows])
    queries = [own_q] + [along_y(own_q, by) for by in Y_SHIFTS[1:]]
    gathered = lax.all_gather(own_kr, "sp_0")
    mine = jnp.concatenate([gathered[:, :32].reshape(NZ * 32, rows), *queries], 0)
    held = [mine] + [along_x(mine, by) for by in X_SHIFTS[1:]]
    held = held + [to_partner(value) for value in held]

    outer, gated = call(
        gates_kernel, (shapes((rows, 128), f32), shapes((rows, 128), bf16)), 2 * 256 * 2048 * 384
    )(pieces, outer_gate, inner_gate, conv_input)
    length = lax.axis_size(SP)
    rim = lax.ppermute(gated[rows - 2 :], SP, [(i, i + 1) for i in range(length - 1)])

    parts = call(
        attention_kernel,
        shapes((NY, HEADS * VDIM + STATS, rows), bf16),
        2 * 1024 * 4096 * 512,
        (
            pltpu.VMEM((HEADS, NY, NOPE + ROPE, rows), bf16),
            pltpu.VMEM((HEADS, CHUNK * rows, NOPE + ROPE), bf16),
            pltpu.VMEM((HEADS, VDIM + 16, CHUNK * rows), bf16),
            pltpu.VMEM((HEADS, NY, VDIM + 16, rows), f32),
            pltpu.VMEM((HEADS, NY, 8, rows), f32),
        ),
        1,
    )(jnp.stack([z, y]).astype(jnp.int32), *held, gathered, wq, wk, gq, gk, cosine, sine)
    merged = lax.all_to_all(parts, "sp_1", 0, 0, tiled=True)
    partial = call(project_kernel, shapes((rows, conv_project.shape[1]), bf16), 2 * 256 * 256 * 2048)(
        merged, outer, gated, rim, conv_taps, conv_project, attend_project
    )
    share = rows // groups
    arrived = lax.all_to_all(
        partial.reshape(groups, share, -1), "tp", split_axis=0, concat_axis=0, tiled=True
    )
    return arrived.astype(f32).sum(axis=0).astype(bf16)


def solution(mesh):
    split = Mesh(mesh.devices.reshape(NZ, NY, mesh.shape["tp"]), ("sp_0", "sp_1", "tp"))
    in_specs = (
        P(SP, "tp"),
        P(None, "tp"),
        P(None, "tp"),
        P(None, "tp"),
        P(None, "tp"),
        P(None, "tp"),
        P(None, "tp"),
        P(),
        P(),
        P(),
        P(None, "tp"),
        P(None, "tp"),
        P("tp", None),
        P("tp", None),
    )
    out_specs = P(SP_TP, None)
    return jax.shard_map(local, mesh=split, in_specs=in_specs, out_specs=out_specs, check_vma=False)
```

time: 447 us -> 157 us (0.35)
  the two profiles are of different devices: /device:TPU:504 before, /device:TPU:384 now
where the time goes in v1:
time: 157 us; the launch traced here: 156 us
  blocking collectives  50 us (32%)
  starting transfers between devices  39.9 us (25%)
  Pallas kernels  29.8 us (19%)
  local copies, waits for them, and re-layouts  16.8 us (11%)
  waiting for transfers between devices  15.8 us (10%)
  other arithmetic  3.28 us (2%)
    all_gather x1, blocking collectives, local(): gathered = lax.all_gather(own_kr, 'sp_0')  31.3 us
    pallas_call x4, Pallas kernels, run(): pl.pallas_call(kernel, out_shape=outs, in_specs=[SMEM] * scalars + [VMEM]...  29.8 us
    all_to_all x1, blocking collectives, local(): lax.all_to_all(partial.reshape(groups, share, -1), 'tp', split_axis=0, co...  18.8 us
    ppermute x3, starting transfers between devices, along_y(): return lax.ppermute(value, 'sp_1', [(i, (i + by) % NY) for i in range(NY)])  10.9 us
    unnamed x53, local copies, waits for them, and re-layouts  9.26 us
    ppermute x3, starting transfers between devices, along_x(): return lax.ppermute(value, 'tp', [(i, (i + 2 * by) % 8) for i in range(8)])  8.97 us
    all_to_all x1, waiting for transfers between devices, local(): pieces = lax.all_to_all(everyone, 'tp', 0, 0, tiled=True)  8.87 us
    ppermute x4, starting transfers between devices, to_partner(): return lax.ppermute(value, 'tp', [(i, i ^ 1) for i in range(8)])  8.14 us
  transfers between devices with their start and end apart: 13, of which 4 were waited for; matrix products, arithmetic and copies ran while one was open for 6% of the time, Pallas kernels for 1%

profile of v1, /device:TPU:384, one launch (start us, length us, event | category | flops | bytes accessed | tf_op | source)
XLA Modules:
  0.0 156.1 jit_solution(11160233532711422793)
XLA Ops:
  0.0 2.0 %broadcast_in_dim.54 = bf16[8,256,256]{2,1,0:T(8,128)(2,1)} broadcast(bf16[256,256]{1,0:T(8,128)(2,1)} %param.16), dimensions={1,2} | broadcast | bytes 1179648 | tf_op jit(solution)/shard_map/broadcast_in_dim | solution.py:248
  2.0 4.3 %all-to-all-start = ((bf16[8,256,256]{2,1,0:T(8,128)(2,1)}), bf16[8,256,256]{2,1,0:T(8,128)(2,1)S(1)}, u32[]{:S(2)}, u32[]{:S(2)}) async-start(bf16[8,256,256]{2,1,0:T(8,128)(2,1)} %broadcast_in_dim.54), calls=%async_computation | async-start | bytes 2097152 | tf_op jit(solution)/shard_map/all_to_all | solution.py:249
  13.3 8.9 %all-to-all-done.tok = bf16[8,256,256]{2,1,0:T(8,128)(2,1)S(1)} async-done(((bf16[8,256,256]{2,1,0:T(8,128)(2,1)}), bf16[8,256,256]{2,1,0:T(8,128)(2,1)S(1)}, u32[]{:S(2)}, u32[]{:S(2)}) %all-to-all-start) | async-done | bytes 1048608 | tf_op jit(solution)/shard_map/all_to_all | solution.py:249
  22.2 1.1 shard_map.154
  23.3 5.1 %collective-permute-start.2 = (bf16[64,256]{1,0:T(8,128)(2,1)S(1)}, bf16[64,256]{1,0:T(8,128)(2,1)S(1)}, u32[]{:S(2)}, u32[]{:S(2)}) collective-permute-start(bf16[64,256]{1,0:T(8,128)(2,1)S(1)} %get-tuple-element.10), channel_id=1, source_target_pairs={{0,16},{8,24},{16,0},{24,8},{1,17},{9,25},{17,1},{25,9},{2,18},{10... | collective-permute-start | bytes 98312 | tf_op jit(solution)/shard_map/ppermute | solution.py:223
  28.4 3.0 %collective-permute-start.1 = (bf16[64,256]{1,0:T(8,128)(2,1)S(1)}, bf16[64,256]{1,0:T(8,128)(2,1)S(1)}, u32[]{:S(2)}, u32[]{:S(2)}) collective-permute-start(bf16[64,256]{1,0:T(8,128)(2,1)S(1)} %get-tuple-element.10), channel_id=1, source_target_pairs={{0,24},{8,0},{16,8},{24,16},{1,25},{9,1},{17,9},{25,17},{2,26},{10... | collective-permute-start | bytes 98312 | tf_op jit(solution)/shard_map/ppermute | solution.py:223
  31.4 2.9 %collective-permute-start = (bf16[64,256]{1,0:T(8,128)(2,1)S(1)}, bf16[64,256]{1,0:T(8,128)(2,1)S(1)}, u32[]{:S(2)}, u32[]{:S(2)}) collective-permute-start(bf16[64,256]{1,0:T(8,128)(2,1)S(1)} %get-tuple-element.10), channel_id=1, source_target_pairs={{0,8},{8,16},{16,24},{24,0},{1,9},{9,17},{17,25},{25,1},{2,10},{10... | collective-permute-start | bytes 98312 | tf_op jit(solution)/shard_map/ppermute | solution.py:223
  34.3 31.3 %all-gather = bf16[1024,256]{1,0:T(8,128)(2,1)S(1)} all-gather(bf16[64,256]{1,0:T(8,128)(2,1)S(1)} %get-tuple-element.9), channel_id=2, replica_groups=mesh['sp_0'=16,'sp_1'=4,'tp'=8] {'sp_0'}, dimensions={0}, use_global_device_ids=true | all-gather | bytes 557056 | tf_op jit(solution)/shard_map/all_gather | solution.py:270
  65.7 2.2 %collective-permute-start.5 = (bf16[768,256]{1,0:T(8,128)(2,1)S(1)}, bf16[768,256]{1,0:T(8,128)(2,1)S(1)}, u32[]{:S(2)}, u32[]{:S(2)}) collective-permute-start(bf16[768,256]{1,0:T(8,128)(2,1)S(1)} %constant_dynamic-update-slice_fusion.refs_0_), channel_id=1, source_target_pairs={{0,4},{1,5},{2,6},{3,7},{4,0},{5,1},{6,2},{7,3},{8,12},{9,13},{10,... | collective-permute-start | bytes 1179656 | tf_op jit(solution)/shard_map/ppermute | solution.py:215
  67.9 4.8 %collective-permute-start.4 = (bf16[768,256]{1,0:T(8,128)(2,1)S(1)}, bf16[768,256]{1,0:T(8,128)(2,1)S(1)}, u32[]{:S(2)}, u32[]{:S(2)}) collective-permute-start(bf16[768,256]{1,0:T(8,128)(2,1)S(1)} %constant_dynamic-update-slice_fusion.refs_0_), channel_id=1, source_target_pairs={{0,6},{1,7},{2,0},{3,1},{4,2},{5,3},{6,4},{7,5},{8,14},{9,15},{10,... | collective-permute-start | bytes 1179656 | tf_op jit(solution)/shard_map/ppermute | solution.py:215
  72.7 1.9 %collective-permute-start.3 = (bf16[768,256]{1,0:T(8,128)(2,1)S(1)}, bf16[768,256]{1,0:T(8,128)(2,1)}, u32[]{:S(2)}, u32[]{:S(2)}) collective-permute-start(bf16[768,256]{1,0:T(8,128)(2,1)S(1)} %constant_dynamic-update-slice_fusion.refs_0_), channel_id=1, source_target_pairs={{0,2},{1,3},{2,4},{3,5},{4,6},{5,7},{6,0},{7,1},{8,10},{9,11},{10,... | collective-permute-start | bytes 1179656 | tf_op jit(solution)/shard_map/ppermute | solution.py:215
  75.4 1.9 %collective-permute-start.6 = (bf16[768,256]{1,0:T(8,128)(2,1)S(1)}, bf16[768,256]{1,0:T(8,128)(2,1)}, u32[]{:S(2)}, u32[]{:S(2)}) collective-permute-start(bf16[768,256]{1,0:T(8,128)(2,1)S(1)} %constant_dynamic-update-slice_fusion.refs_0_), channel_id=1, source_target_pairs={{0,1},{1,0},{2,3},{3,2},{4,5},{5,4},{6,7},{7,6},{8,9},{9,8},{10,11... | collective-permute-start | bytes 1179656 | tf_op jit(solution)/shard_map/ppermute | solution.py:219
  77.6 2.2 %collective-permute-start.9 = (bf16[768,256]{1,0:T(8,128)(2,1)S(1)}, bf16[768,256]{1,0:T(8,128)(2,1)}, u32[]{:S(2)}, u32[]{:S(2)}) collective-permute-start(bf16[768,256]{1,0:T(8,128)(2,1)S(1)} %collective-permute-done.5.refs_3_), channel_id=1, source_target_pairs={{0,1},{1,0},{2,3},{3,2},{4,5},{5,4},{6,7},{7,6},{8,9},{9,8},{10,11... | collective-permute-start | bytes 1179656 | tf_op jit(solution)/shard_map/ppermute | solution.py:219
  79.8 2.2 %collective-permute-start.8 = (bf16[768,256]{1,0:T(8,128)(2,1)S(1)}, bf16[768,256]{1,0:T(8,128)(2,1)}, u32[]{:S(2)}, u32[]{:S(2)}) collective-permute-start(bf16[768,256]{1,0:T(8,128)(2,1)S(1)} %collective-permute-done.4.refs_2_), channel_id=1, source_target_pairs={{0,1},{1,0},{2,3},{3,2},{4,5},{5,4},{6,7},{7,6},{8,9},{9,8},{10,11... | collective-permute-start | bytes 1179656 | tf_op jit(solution)/shard_map/ppermute | solution.py:219
  82.0 1.8 %collective-permute-done.3.refs_1_ = bf16[768,256]{1,0:T(8,128)(2,1)} collective-permute-done((bf16[768,256]{1,0:T(8,128)(2,1)S(1)}, bf16[768,256]{1,0:T(8,128)(2,1)}, u32[]{:S(2)}, u32[]{:S(2)}) %collective-permute-start.3) | collective-permute-done | bytes 393248 | tf_op jit(solution)/shard_map/ppermute | solution.py:215
  83.7 1.9 %collective-permute-start.7 = (bf16[768,256]{1,0:T(8,128)(2,1)}, bf16[768,256]{1,0:T(8,128)(2,1)}, u32[]{:S(2)}, u32[]{:S(2)}) collective-permute-start(bf16[768,256]{1,0:T(8,128)(2,1)} %collective-permute-done.3.refs_1_), channel_id=1, source_target_pairs={{0,1},{1,0},{2,3},{3,2},{4,5},{5,4},{6,7},{7,6},{8,9},{9,8},{10,11... | collective-permute-start | bytes 1179656 | tf_op jit(solution)/shard_map/ppermute | solution.py:219
  87.7 1.5 gather_fusion
  93.2 27.2 %shard_map.155 = bf16[4,144,256]{2,1,0:T(8,128)(2,1)} custom-call(s32[2]{0:T(128)S(1)} %pad_add_fusion.where, bf16[768,256]{1,0:T(8,128)(2,1)S(1)} %constant_dynamic-update-slice_fusion.refs_0_, bf16[768,256]{1,0:T(8,128)(2,1)} %collective-permute-done.3.refs_1_, bf16[768,256]{1,0:T(8,128)(2,1)S(1)} %copy-done.14, bf16[768,256]{1,0:T(8,128)(2,1)S(1)} %copy-done.12, ...), custom_call_target="tpu_custom_call" | custom-call | flops 4294967296 | bytes 4194304 | tf_op jit(solution)/shard_map/pallas_call | solution.py:201
  120.4 3.7 %all-to-all-start.1 = ((bf16[4,144,256]{2,1,0:T(8,128)(2,1)}), bf16[4,144,256]{2,1,0:T(8,128)(2,1)S(1)}, u32[]{:S(2)}, u32[]{:S(2)}) async-start(bf16[4,144,256]{2,1,0:T(8,128)(2,1)} %shard_map.155), calls=%async_computation.1 | async-start | bytes 589824 | tf_op jit(solution)/shard_map/all_to_all | solution.py:294
  125.1 3.9 %collective-permute-start.10 = (bf16[2,128]{1,0:T(2,128)(2,1)S(1)}, bf16[2,128]{1,0:T(2,128)(2,1)S(1)}, u32[]{:S(2)}, u32[]{:S(2)}) collective-permute-start(bf16[2,128]{1,0:T(2,128)(2,1)S(1)} %slice.15), channel_id=1, source_target_pairs={{0,8},{8,16},{16,24},{24,32},{32,40},{40,48},{48,56},{56,64},{64,7... | collective-permute-start | bytes 1544 | tf_op jit(solution)/shard_map/ppermute | solution.py:279
  129.0 4.8 %collective-permute-done.10.rim = bf16[2,128]{1,0:T(2,128)(2,1)S(1)} collective-permute-done((bf16[2,128]{1,0:T(2,128)(2,1)S(1)}, bf16[2,128]{1,0:T(2,128)(2,1)S(1)}, u32[]{:S(2)}, u32[]{:S(2)}) %collective-permute-start.10) | collective-permute-done | bytes 544 | tf_op jit(solution)/shard_map/ppermute | solution.py:279
  133.9 1.0 copy-done.4
  134.9 1.0 copy-done.5
  136.5 18.8 %all_to_all.15 = bf16[8,32,2048]{2,1,0:T(8,128)(2,1)S(1)} all-to-all(bf16[8,32,2048]{2,1,0:T(8,128)(2,1)S(1)} %bitcast.22), channel_id=1, replica_groups=mesh['sp_0'=16,'sp_1'=4,'tp'=8] {'tp'}, dimensions={0} | all-to-all | bytes 2097152 | tf_op jit(solution)/shard_map/all_to_all | solution.py:299
  (96 shorter events, 16.3 us)
Async XLA Ops:
  0.0 10.3 %copy-start = (bf16[256,256]{1,0:T(8,128)(2,1)S(1)}, bf16[256,256]{1,0:T(8,128)(2,1)}, u32[]{:S(2)}) copy-start(bf16[256,256]{1,0:T(8,128)(2,1)} %param.27) | copy-start | bytes 393220
  2.0 20.2 %all-to-all-start = ((bf16[8,256,256]{2,1,0:T(8,128)(2,1)}), bf16[8,256,256]{2,1,0:T(8,128)(2,1)S(1)}, u32[]{:S(2)}, u32[]{:S(2)}) async-start(bf16[8,256,256]{2,1,0:T(8,128)(2,1)} %broadcast_in_dim.54), calls=%async_computation | async-start | bytes 2097152 | tf_op jit(solution)/shard_map/all_to_all | solution.py:249
  23.3 42.3 %collective-permute-start.2 = (bf16[64,256]{1,0:T(8,128)(2,1)S(1)}, bf16[64,256]{1,0:T(8,128)(2,1)S(1)}, u32[]{:S(2)}, u32[]{:S(2)}) collective-permute-start(bf16[64,256]{1,0:T(8,128)(2,1)S(1)} %get-tuple-element.10), channel_id=1, source_target_pairs={{0,16},{8,24},{16,0},{24,8},{1,17},{9,25},{17,1},{25,9},{2,18},{10... | collective-permute-start | bytes 98312 | tf_op jit(solution)/shard_map/ppermute | solution.py:223
  28.4 37.2 %collective-permute-start.1 = (bf16[64,256]{1,0:T(8,128)(2,1)S(1)}, bf16[64,256]{1,0:T(8,128)(2,1)S(1)}, u32[]{:S(2)}, u32[]{:S(2)}) collective-permute-start(bf16[64,256]{1,0:T(8,128)(2,1)S(1)} %get-tuple-element.10), channel_id=1, source_target_pairs={{0,24},{8,0},{16,8},{24,16},{1,25},{9,1},{17,9},{25,17},{2,26},{10... | collective-permute-start | bytes 98312 | tf_op jit(solution)/shard_map/ppermute | solution.py:223
  31.4 34.2 %collective-permute-start = (bf16[64,256]{1,0:T(8,128)(2,1)S(1)}, bf16[64,256]{1,0:T(8,128)(2,1)S(1)}, u32[]{:S(2)}, u32[]{:S(2)}) collective-permute-start(bf16[64,256]{1,0:T(8,128)(2,1)S(1)} %get-tuple-element.10), channel_id=1, source_target_pairs={{0,8},{8,16},{16,24},{24,0},{1,9},{9,17},{17,25},{25,1},{2,10},{10... | collective-permute-start | bytes 98312 | tf_op jit(solution)/shard_map/ppermute | solution.py:223
  65.7 11.9 %collective-permute-start.5 = (bf16[768,256]{1,0:T(8,128)(2,1)S(1)}, bf16[768,256]{1,0:T(8,128)(2,1)S(1)}, u32[]{:S(2)}, u32[]{:S(2)}) collective-permute-start(bf16[768,256]{1,0:T(8,128)(2,1)S(1)} %constant_dynamic-update-slice_fusion.refs_0_), channel_id=1, source_target_pairs={{0,4},{1,5},{2,6},{3,7},{4,0},{5,1},{6,2},{7,3},{8,12},{9,13},{10,... | collective-permute-start | bytes 1179656 | tf_op jit(solution)/shard_map/ppermute | solution.py:215
  67.9 11.9 %collective-permute-start.4 = (bf16[768,256]{1,0:T(8,128)(2,1)S(1)}, bf16[768,256]{1,0:T(8,128)(2,1)S(1)}, u32[]{:S(2)}, u32[]{:S(2)}) collective-permute-start(bf16[768,256]{1,0:T(8,128)(2,1)S(1)} %constant_dynamic-update-slice_fusion.refs_0_), channel_id=1, source_target_pairs={{0,6},{1,7},{2,0},{3,1},{4,2},{5,3},{6,4},{7,5},{8,14},{9,15},{10,... | collective-permute-start | bytes 1179656 | tf_op jit(solution)/shard_map/ppermute | solution.py:215
  72.7 11.0 %collective-permute-start.3 = (bf16[768,256]{1,0:T(8,128)(2,1)S(1)}, bf16[768,256]{1,0:T(8,128)(2,1)}, u32[]{:S(2)}, u32[]{:S(2)}) collective-permute-start(bf16[768,256]{1,0:T(8,128)(2,1)S(1)} %constant_dynamic-update-slice_fusion.refs_0_), channel_id=1, source_target_pairs={{0,2},{1,3},{2,4},{3,5},{4,6},{5,7},{6,0},{7,1},{8,10},{9,11},{10,... | collective-permute-start | bytes 1179656 | tf_op jit(solution)/shard_map/ppermute | solution.py:215
  75.4 15.7 %collective-permute-start.6 = (bf16[768,256]{1,0:T(8,128)(2,1)S(1)}, bf16[768,256]{1,0:T(8,128)(2,1)}, u32[]{:S(2)}, u32[]{:S(2)}) collective-permute-start(bf16[768,256]{1,0:T(8,128)(2,1)S(1)} %constant_dynamic-update-slice_fusion.refs_0_), channel_id=1, source_target_pairs={{0,1},{1,0},{2,3},{3,2},{4,5},{5,4},{6,7},{7,6},{8,9},{9,8},{10,11... | collective-permute-start | bytes 1179656 | tf_op jit(solution)/shard_map/ppermute | solution.py:219
  77.6 10.1 %copy-start.11 = (bf16[768,256]{1,0:T(8,128)(2,1)}, bf16[768,256]{1,0:T(8,128)(2,1)S(1)}, u32[]{:S(2)}) copy-start(bf16[768,256]{1,0:T(8,128)(2,1)S(1)} %collective-permute-done.5.refs_3_) | copy-start | bytes 1179652
  77.6 13.5 %collective-permute-start.9 = (bf16[768,256]{1,0:T(8,128)(2,1)S(1)}, bf16[768,256]{1,0:T(8,128)(2,1)}, u32[]{:S(2)}, u32[]{:S(2)}) collective-permute-start(bf16[768,256]{1,0:T(8,128)(2,1)S(1)} %collective-permute-done.5.refs_3_), channel_id=1, source_target_pairs={{0,1},{1,0},{2,3},{3,2},{4,5},{5,4},{6,7},{7,6},{8,9},{9,8},{10,11... | collective-permute-start | bytes 1179656 | tf_op jit(solution)/shard_map/ppermute | solution.py:219
  79.8 7.9 %copy-start.13 = (bf16[768,256]{1,0:T(8,128)(2,1)}, bf16[768,256]{1,0:T(8,128)(2,1)S(1)}, u32[]{:S(2)}) copy-start(bf16[768,256]{1,0:T(8,128)(2,1)S(1)} %collective-permute-done.4.refs_2_) | copy-start | bytes 1179652
  79.8 11.4 %collective-permute-start.8 = (bf16[768,256]{1,0:T(8,128)(2,1)S(1)}, bf16[768,256]{1,0:T(8,128)(2,1)}, u32[]{:S(2)}, u32[]{:S(2)}) collective-permute-start(bf16[768,256]{1,0:T(8,128)(2,1)S(1)} %collective-permute-done.4.refs_2_), channel_id=1, source_target_pairs={{0,1},{1,0},{2,3},{3,2},{4,5},{5,4},{6,7},{7,6},{8,9},{9,8},{10,11... | collective-permute-start | bytes 1179656 | tf_op jit(solution)/shard_map/ppermute | solution.py:219
  83.7 7.4 %collective-permute-start.7 = (bf16[768,256]{1,0:T(8,128)(2,1)}, bf16[768,256]{1,0:T(8,128)(2,1)}, u32[]{:S(2)}, u32[]{:S(2)}) collective-permute-start(bf16[768,256]{1,0:T(8,128)(2,1)} %collective-permute-done.3.refs_1_), channel_id=1, source_target_pairs={{0,1},{1,0},{2,3},{3,2},{4,5},{5,4},{6,7},{7,6},{8,9},{9,8},{10,11... | collective-permute-start | bytes 1179656 | tf_op jit(solution)/shard_map/ppermute | solution.py:219
  90.1 1.0 copy-start.6
  90.1 1.1 copy-start.7
  90.1 1.1 copy-start.9
  93.2 30.9 %copy-start.2 = (bf16[2048,128]{1,0:T(8,128)(2,1)S(1)}, bf16[2048,128]{1,0:T(8,128)(2,1)}, u32[]{:S(2)}) copy-start(bf16[2048,128]{1,0:T(8,128)(2,1)} %wi.1) | copy-start | bytes 1572868
  93.2 30.9 %copy-start.3 = (bf16[2048,128]{1,0:T(8,128)(2,1)S(1)}, bf16[2048,128]{1,0:T(8,128)(2,1)}, u32[]{:S(2)}) copy-start(bf16[2048,128]{1,0:T(8,128)(2,1)} %ws.1) | copy-start | bytes 1572868
  120.4 3.7 %copy-start.1 = (bf16[2048,128]{1,0:T(8,128)(2,1)S(1)}, bf16[2048,128]{1,0:T(8,128)(2,1)}, u32[]{:S(2)}) copy-start(bf16[2048,128]{1,0:T(8,128)(2,1)} %wo.1) | copy-start | bytes 1572868
  120.4 13.4 %all-to-all-start.1 = ((bf16[4,144,256]{2,1,0:T(8,128)(2,1)}), bf16[4,144,256]{2,1,0:T(8,128)(2,1)S(1)}, u32[]{:S(2)}, u32[]{:S(2)}) async-start(bf16[4,144,256]{2,1,0:T(8,128)(2,1)} %shard_map.155), calls=%async_computation.1 | async-start | bytes 589824 | tf_op jit(solution)/shard_map/all_to_all | solution.py:294
  125.1 8.8 %copy-start.10 = (bf16[3,128]{1,0:T(4,128)(2,1)S(1)}, bf16[3,128]{1,0:T(4,128)(2,1)}, u32[]{:S(2)}) copy-start(bf16[3,128]{1,0:T(4,128)(2,1)} %taps.1) | copy-start | bytes 2308
  125.1 8.8 %collective-permute-start.10 = (bf16[2,128]{1,0:T(2,128)(2,1)S(1)}, bf16[2,128]{1,0:T(2,128)(2,1)S(1)}, u32[]{:S(2)}, u32[]{:S(2)}) collective-permute-start(bf16[2,128]{1,0:T(2,128)(2,1)S(1)} %slice.15), channel_id=1, source_target_pairs={{0,8},{8,16},{16,24},{24,32},{32,40},{40,48},{48,56},{56,64},{64,7... | collective-permute-start | bytes 1544 | tf_op jit(solution)/shard_map/ppermute | solution.py:279
  133.9 1.0 copy-start.4
  (11 other events, 9.4 us)
